TPU v7x, 32 devices: a whole 2x2x4 slice. The times are simulated.
32 devices in a mesh: rep: 2 (over x), fs: 4 (over z), tp: 4 (over y, core).
Axes of the slice: x: 2, y: 2, z: 4, core: 2. Of those that a mesh axis runs over, the one named last changes fastest.
Arguments:
- tokens: bfloat16 [4096, 1024], P(('rep', 'fs', 'tp')), may hold values from -6 to 6
- w_up: bfloat16 [1024, 4096], P('fs', 'tp'), may hold values from -0.1875 to 0.1875
- w_down: bfloat16 [4096, 1024], P('tp', 'fs'), may hold values from -0.09375 to 0.09375
- out_gain: float32 [1024], replicated, may hold values from 0.1 to 1.9
- out_shift: float32 [1024], replicated, may hold values from -3 to 3
Outputs:
- normed: bfloat16 [4096, 1024], P(('rep', 'fs', 'tp'))
All inputs are finite; a program needn't handle non-finite values.
Results may differ from a plain program's by a relative error of at most 0.015.
Values may be sent and summed in bfloat16 or wider, within the bound.
A program may use at most 64 MiB of HBM per device.

v0:
```python
import jax
import jax.numpy as jnp
from jax import lax
from jax.sharding import PartitionSpec as P

residual_scale = 2.0**0.25
norm_eps = 1e-05


def over_all(share, axis, dim, apply):
    everything = lax.all_gather(share, axis, axis=dim, tiled=True)
    return apply(everything, jnp.int32(0))


def summed_rows(product, extent, axis):
    whole = product(jnp.int32(0), extent * lax.axis_size(axis)).astype(jnp.bfloat16)
    return lax.psum_scatter(whole, axis, scatter_dimension=0, tiled=True).astype(jnp.float32)


def layer_norm(summed, out_gain, out_shift):
    row_mean = jnp.mean(summed, axis=-1, keepdims=True)
    centered = summed - row_mean
    row_var = jnp.mean(centered * centered, axis=-1, keepdims=True)
    return centered * lax.rsqrt(row_var + norm_eps) * out_gain + out_shift


def squared_relu(pre_act):
    return jnp.square(jnp.maximum(pre_act, 0.0)).astype(jnp.bfloat16)


def shards(tokens, w_up, w_down, out_gain, out_shift):
    up_block = lax.all_gather(w_up, "fs", axis=0, tiled=True)

    def activate(block_rows, offset):
        return squared_relu(jnp.dot(block_rows, up_block, preferred_element_type=jnp.float32))

    hidden = over_all(tokens, "tp", 0, activate)
    down_block = lax.all_gather(w_down, "fs", axis=1, tiled=True)
    own_count = tokens.shape[0]

    def project(offset, how_many):
        picked = lax.dynamic_slice_in_dim(hidden, offset, how_many, 0)
        return jnp.dot(picked, down_block, preferred_element_type=jnp.float32)

    branch = summed_rows(project, own_count, "tp")
    summed = residual_scale * tokens.astype(jnp.float32) + branch
    return layer_norm(summed, out_gain, out_shift).astype(jnp.bfloat16)


def solution(mesh):
    in_specs = (P(("rep", "fs", "tp"), None), P("fs", "tp"), P("tp", "fs"), P(), P())
    out_specs = P(("rep", "fs", "tp"), None)
    return jax.shard_map(shards, mesh=mesh, in_specs=in_specs, out_specs=out_specs, check_vma=False)
```

profile of v0, /device:TPU:0, one launch (start us, length us, event | category | flops | bytes accessed | tf_op | source)
XLA Modules:
  0.0 162.0 jit_solution(3515093248988575749)
XLA Ops:
  6.5 0.0 all-gather.4.cloned.1.call-start
  6.5 0.7 all-gather.4.cloned.1.call-update
  7.3 0.0 all-gather.6.cloned.1.call-start
  7.3 0.7 all-gather.6.cloned.1.call-update
  8.0 0.0 all-gather.8.cloned.1.call-start
  8.1 0.7 all-gather.8.cloned.1.call-update
  8.7 0.0 copy-start
  8.8 0.0 reduce-scatter.2.cloned.1.call-start
  8.8 19.6 %all-gather.4.cloned.1.call-done = bf16[512,1024]{1,0:T(8,128)(2,1)} async-done(((bf16[128,1024]{1,0:T(8,128)(2,1)}), bf16[512,1024]{1,0:T(8,128)(2,1)}) %all-gather.4.cloned.1.call-update) | async-done | bytes 1048592 | tf_op jit(solution)/shard_map/all_gather | solution.py:11
  28.3 47.3 %all-gather.6.cloned.1.call-done = bf16[1024,1024]{1,0:T(8,128)(2,1)} async-done(((bf16[256,1024]{1,0:T(8,128)(2,1)}), bf16[1024,1024]{1,0:T(8,128)(2,1)}) %all-gather.6.cloned.1.call-update) | async-done | bytes 2097168 | tf_op jit(solution)/shard_map/all_gather | solution.py:32
  75.6 46.7 %all-gather.8.cloned.1.call-done = bf16[1024,1024]{1,0:T(8,128)(2,1)} async-done(((bf16[1024,256]{1,0:T(8,128)(2,1)}), bf16[1024,1024]{1,0:T(8,128)(2,1)}) %all-gather.8.cloned.1.call-update) | async-done | bytes 2097168 | tf_op jit(solution)/shard_map/all_gather | solution.py:38
  122.3 5.8 %convolution_convert_fusion = bf16[512,1024]{1,0:T(8,128)(2,1)} fusion(bf16[1024,1024]{1,0:T(8,128)(2,1)} %all-gather.8.cloned.1.call-done, bf16[512,1024]{1,0:T(8,128)(2,1)} %all-gather.4.cloned.1.call-done, bf16[1024,1024]{1,0:T(8,128)(2,1)} %all-gather.6.cloned.1.call-done), kind=kOutput, calls=%fused_computation.1 | convolution fusion | flops 2149580800 | bytes 6291456 | tf_op jit(solution)/shard_map/dot_general | solution.py:43
  128.1 0.0 copy-start.1
  128.1 0.0 copy-start.2
  128.1 0.0 reduce-scatter.2.cloned.1.call-update
  128.1 23.2 %reduce-scatter.2.cloned.1.call-done = bf16[128,1024]{1,0:T(8,128)(2,1)} async-done(((bf16[512,1024]{1,0:T(8,128)(2,1)}), bf16[128,1024]{1,0:T(8,128)(2,1)}) %reduce-scatter.2.cloned.1.call-update) | async-done | bytes 262160 | tf_op jit(solution)/shard_map/reduce_scatter | solution.py:17
  151.3 0.0 copy-done
  151.3 1.1 fusion
  152.4 1.2 multiply_reduce_fusion
  153.6 0.0 copy-done.1
  153.6 0.0 copy-done.2
  153.6 1.8 %add_convert_fusion = bf16[128,1024]{1,0:T(8,128)(2,1)} fusion(bf16[128,1024]{1,0:T(8,128)(2,1)} %reduce-scatter.2.cloned.1.call-done, bf16[128,1024]{1,0:T(8,128)(2,1)S(1)} %copy-done, f32[1024]{0:T(1024)S(1)} %copy-done.1, f32[1024]{0:T(1024)S(1)} %copy-done.2, f32[128]{0:T(128)S(1)} %add_rsqrt_fusion, f32[128]{0:T(128)S(1)} %broadcast_multiply_fusion), kind=kLoop, calls=%fused_computation.2 | loop fusion | flops 1179648 | bytes 795648 | tf_op jit(solution)/shard_map/convert_element_type | solution.py:47
  (2 shorter events, 0.0 us)
Async XLA Ops:
  6.5 21.8 %all-gather.4.cloned.1.call-start = ((), (), s32[]{:S(2)}) async-start(), calls=%async_computation.1 | async-start | bytes 1310720 | tf_op jit(solution)/shard_map/all_gather | solution.py:11
  7.3 68.3 %all-gather.6.cloned.1.call-start = ((), (), s32[]{:S(2)}) async-start(), calls=%async_computation.2 | async-start | bytes 2621440 | tf_op jit(solution)/shard_map/all_gather | solution.py:32
  8.0 114.3 %all-gather.8.cloned.1.call-start = ((), (), s32[]{:S(2)}) async-start(), calls=%async_computation.3 | async-start | bytes 2621440 | tf_op jit(solution)/shard_map/all_gather | solution.py:38
  8.7 142.6 %copy-start = (bf16[128,1024]{1,0:T(8,128)(2,1)S(1)}, bf16[128,1024]{1,0:T(8,128)(2,1)}, u32[]{:S(2)}) copy-start(bf16[128,1024]{1,0:T(8,128)(2,1)} %param.5) | copy-start | bytes 786436
  8.8 142.6 %reduce-scatter.2.cloned.1.call-start = ((), (), s32[]{:S(2)}) async-start(), calls=%async_computation.4 | async-start | bytes 1310720 | tf_op jit(solution)/shard_map/reduce_scatter | solution.py:17
  128.1 25.5 %copy-start.1 = (f32[1024]{0:T(1024)S(1)}, f32[1024]{0:T(1024)}, u32[]{:S(2)}) copy-start(f32[1024]{0:T(1024)} %param.9) | copy-start | bytes 12292
  128.1 25.5 %copy-start.2 = (f32[1024]{0:T(1024)S(1)}, f32[1024]{0:T(1024)}, u32[]{:S(2)}) copy-start(f32[1024]{0:T(1024)} %param.8) | copy-start | bytes 12292
Sparse Core Ops, SparseCore 0:
  8.9 19.4 all-gather.3
  29.9 45.6 all-gather.5
  77.2 45.0 all-gather.7
  128.3 22.9 reduce-scatter.1
where the time goes:
time: 162 us
  waiting for transfers between devices  139 us (86%)
  between operations  13.2 us (8%)
  matrix products  5.85 us (4%)
  other arithmetic  4.1 us (3%)
    all_gather x1, waiting for transfers between devices, shards(): up_block = lax.all_gather(w_up, 'fs', axis=0, tiled=True)  47.3 us
    all_gather x1, waiting for transfers between devices, shards(): down_block = lax.all_gather(w_down, 'fs', axis=1, tiled=True)  46.7 us
    reduce_scatter x1, waiting for transfers between devices, summed_rows(): lax.psum_scatter(whole, axis, scatter_dimension=0, tiled=True)  23.2 us
    all_gather x1, waiting for transfers between devices, over_all(): everything = lax.all_gather(share, axis, axis=dim, tiled=True)  19.6 us
    dot_general x1, matrix products, project(): return jnp.dot(picked, down_block, preferred_element_type=jnp.float32)  5.85 us
  transfers between devices with their start and end apart: 4, of which 4 were waited for; matrix products, arithmetic and copies ran while one was open for 0% of the time, Pallas kernels for 0%

commit v1 on v0

--- a/solution.py
+++ b/solution.py
@@ -29,7 +29,12 @@
 
 
 def shards(tokens, w_up, w_down, out_gain, out_shift):
-    up_block = lax.all_gather(w_up, "fs", axis=0, tiled=True)
+    ring = [w_up]
+    for hop in range(3):
+        ring.append(lax.ppermute(ring[-1], "fs", [(dev, (dev + 1) % 4) for dev in range(4)]))
+    up_block = jnp.roll(
+        jnp.concatenate(ring[::-1], axis=0), (lax.axis_index("fs") + 1) * ring[0].shape[0], axis=0
+    )
 
     def activate(block_rows, offset):
         return squared_relu(jnp.dot(block_rows, up_block, preferred_element_type=jnp.float32))

time: 162 us -> 127 us (0.78)
  waiting for transfers between devices: 139 us -> 94.1 us
  local copies, waits for them, and re-layouts: 0.01 us -> 6.65 us
  starting transfers between devices: 0.12 us -> 3.19 us
    ppermute x0 -> x3, waiting for transfers between devices: none -> 56 us  [shards(): lax.ppermute(ring[-1], 'fs', [(dev, (dev + 1) % 4) for dev in range(4)])]
    all_gather x1 -> x0, waiting for transfers between devices: 47.3 us -> none  [shards(): up_block = lax.all_gather(w_up, 'fs', axis=0, tiled=True)]
    all_gather x1, waiting for transfers between devices: 46.7 us -> 13.6 us  [shards(): down_block = lax.all_gather(w_down, 'fs', axis=1, tiled=True)]
    all_gather x1, waiting for transfers between devices: 19.6 us -> 0.01 us  [over_all(): everything = lax.all_gather(share, axis, axis=dim, tiled=True)]
    unnamed x6 -> x15, local copies, waits for them, and re-layouts: 0.01 us -> 5.83 us
    ppermute x0 -> x3, starting transfers between devices: none -> 3.11 us  [shards(): lax.ppermute(ring[-1], 'fs', [(dev, (dev + 1) % 4) for dev in range(4)])]
  transfers between devices with their start and end apart: 4 -> 6, of which waited for: 4 -> 5; matrix products, arithmetic and copies ran while one was open for 0% -> 5% of each run, Pallas kernels for 0% -> 0%
where the time goes in v1:
time: 127 us
  waiting for transfers between devices  94.1 us (74%)
  between operations  13.1 us (10%)
  local copies, waits for them, and re-layouts  6.65 us (5%)
  matrix products  5.94 us (5%)
  other arithmetic  4.1 us (3%)
  starting transfers between devices  3.19 us (3%)
    ppermute x3, waiting for transfers between devices, shards(): lax.ppermute(ring[-1], 'fs', [(dev, (dev + 1) % 4) for dev in range(4)])  56 us
    reduce_scatter x1, waiting for transfers between devices, summed_rows(): lax.psum_scatter(whole, axis, scatter_dimension=0, tiled=True)  23.1 us
    all_gather x1, waiting for transfers between devices, shards(): down_block = lax.all_gather(w_down, 'fs', axis=1, tiled=True)  13.6 us
    dot_general x1, matrix products, project(): return jnp.dot(picked, down_block, preferred_element_type=jnp.float32)  5.94 us
    unnamed x15, local copies, waits for them, and re-layouts  5.83 us
    ppermute x3, starting transfers between devices, shards(): lax.ppermute(ring[-1], 'fs', [(dev, (dev + 1) % 4) for dev in range(4)])  3.11 us
  transfers between devices with their start and end apart: 6, of which 5 were waited for; matrix products, arithmetic and copies ran while one was open for 5% of the time, Pallas kernels for 0%

profile of v1, /device:TPU:0, one launch (start us, length us, event | category | flops | bytes accessed | tf_op | source)
XLA Modules:
  0.0 127.1 jit_solution(9876476326070030130)
XLA Ops:
  6.5 0.0 copy-start.1
  6.5 0.0 all-gather.3.cloned.1.call-start
  6.5 0.7 all-gather.3.cloned.1.call-update
  7.3 0.0 all-gather.5.cloned.1.call-start
  7.3 0.7 all-gather.5.cloned.1.call-update
  8.0 0.0 reduce-scatter.2.cloned.1.call-start
  8.1 3.1 %collective-permute-start = (bf16[256,1024]{1,0:T(8,128)(2,1)}, bf16[256,1024]{1,0:T(8,128)(2,1)S(1)}, u32[]{:S(2)}, u32[]{:S(2)}) collective-permute-start(bf16[256,1024]{1,0:T(8,128)(2,1)} %param.6), channel_id=1, source_target_pairs={{0,4},{4,8},{8,12},{12,0},{1,5},{5,9},{9,13},{13,1},{2,6},{6,10},{... | collective-permute-start | bytes 1572872 | tf_op jit(solution)/shard_map/ppermute | solution.py:34
  11.2 14.2 %collective-permute-done = bf16[256,1024]{1,0:T(8,128)(2,1)S(1)} collective-permute-done((bf16[256,1024]{1,0:T(8,128)(2,1)}, bf16[256,1024]{1,0:T(8,128)(2,1)S(1)}, u32[]{:S(2)}, u32[]{:S(2)}) %collective-permute-start) | collective-permute-done | bytes 524320 | tf_op jit(solution)/shard_map/ppermute | solution.py:34
  25.3 0.0 collective-permute-start.1
  25.3 14.9 %collective-permute-done.1 = bf16[256,1024]{1,0:T(8,128)(2,1)S(1)} collective-permute-done((bf16[256,1024]{1,0:T(8,128)(2,1)S(1)}, bf16[256,1024]{1,0:T(8,128)(2,1)S(1)}, u32[]{:S(2)}, u32[]{:S(2)}) %collective-permute-start.1) | collective-permute-done | bytes 524320 | tf_op jit(solution)/shard_map/ppermute | solution.py:34
  40.2 0.0 collective-permute-start.2
  40.2 26.9 %collective-permute-done.2 = bf16[256,1024]{1,0:T(8,128)(2,1)S(1)} collective-permute-done((bf16[256,1024]{1,0:T(8,128)(2,1)S(1)}, bf16[256,1024]{1,0:T(8,128)(2,1)S(1)}, u32[]{:S(2)}, u32[]{:S(2)}) %collective-permute-start.2) | collective-permute-done | bytes 524320 | tf_op jit(solution)/shard_map/ppermute | solution.py:34
  67.1 0.8 constant_dynamic-update-slice_fusion.7
  68.0 0.8 constant_dynamic-update-slice_fusion.6
  68.8 0.8 constant_dynamic-update-slice_fusion.5
  69.6 0.0 copy-done.1
  69.6 0.8 constant_dynamic-update-slice_fusion.4
  70.5 0.8 constant_dynamic-update-slice_fusion.3
  71.3 0.8 constant_dynamic-update-slice_fusion.2
  72.1 0.8 constant_dynamic-update-slice_fusion.1
  73.0 0.8 constant_dynamic-update-slice_fusion
  73.8 0.0 copy-start
  73.8 0.0 copy-start.2
  73.8 0.0 copy-start.3
  73.8 0.0 all-gather.3.cloned.1.call-done
  73.8 13.6 %all-gather.5.cloned.1.call-done = bf16[1024,1024]{1,0:T(8,128)(2,1)} async-done(((bf16[1024,256]{1,0:T(8,128)(2,1)}), bf16[1024,1024]{1,0:T(8,128)(2,1)}) %all-gather.5.cloned.1.call-update) | async-done | bytes 2097168 | tf_op jit(solution)/shard_map/all_gather | solution.py:43
  87.4 5.9 %convolution_convert_fusion = bf16[512,1024]{1,0:T(8,128)(2,1)} fusion(bf16[1024,1024]{1,0:T(8,128)(2,1)} %all-gather.5.cloned.1.call-done, bf16[512,1024]{1,0:T(8,128)(2,1)} %all-gather.3.cloned.1.call-done, bf16[2048,1024]{1,0:T(8,128)(2,1)} %constant_dynamic-update-slice_fusion, s32[]{:T(128)S(6)} %select_n.14), kind=kOutput, calls=%fused_computation.3 | convolution fusion | flops 2149580800 | bytes 6291460 | tf_op jit(solution)/shard_map/dot_general | solution.py:48
  93.4 0.0 reduce-scatter.2.cloned.1.call-update
  93.4 23.1 %reduce-scatter.2.cloned.1.call-done = bf16[128,1024]{1,0:T(8,128)(2,1)} async-done(((bf16[512,1024]{1,0:T(8,128)(2,1)}), bf16[128,1024]{1,0:T(8,128)(2,1)}) %reduce-scatter.2.cloned.1.call-update) | async-done | bytes 262160 | tf_op jit(solution)/shard_map/reduce_scatter | solution.py:17
  116.5 0.0 copy-done
  116.5 1.1 fusion.6
  117.6 1.2 multiply_reduce_fusion
  118.8 0.0 copy-done.2
  118.8 0.0 copy-done.3
  118.8 1.8 %add_convert_fusion = bf16[128,1024]{1,0:T(8,128)(2,1)} fusion(bf16[128,1024]{1,0:T(8,128)(2,1)} %reduce-scatter.2.cloned.1.call-done, bf16[128,1024]{1,0:T(8,128)(2,1)S(1)} %copy-done, f32[1024]{0:T(1024)S(1)} %copy-done.2, f32[1024]{0:T(1024)S(1)} %copy-done.3, f32[128]{0:T(128)S(1)} %add_rsqrt_fusion, f32[128]{0:T(128)S(1)} %broadcast_multiply_fusion), kind=kLoop, calls=%fused_computation.4 | loop fusion | flops 1179648 | bytes 795648 | tf_op jit(solution)/shard_map/convert_element_type | solution.py:52
  (2 shorter events, 0.0 us)
Async XLA Ops:
  6.5 63.1 %copy-start.1 = (bf16[256,1024]{1,0:T(8,128)(2,1)S(1)}, bf16[256,1024]{1,0:T(8,128)(2,1)}, u32[]{:S(2)}) copy-start(bf16[256,1024]{1,0:T(8,128)(2,1)} %param.6) | copy-start | bytes 1572868
  6.5 67.2 %all-gather.3.cloned.1.call-start = ((), (), s32[]{:S(2)}) async-start(), calls=%async_computation.1 | async-start | bytes 1310720 | tf_op jit(solution)/shard_map/all_gather | solution.py:11
  7.3 80.2 %all-gather.5.cloned.1.call-start = ((), (), s32[]{:S(2)}) async-start(), calls=%async_computation.2 | async-start | bytes 2621440 | tf_op jit(solution)/shard_map/all_gather | solution.py:43
  8.0 108.5 %reduce-scatter.2.cloned.1.call-start = ((), (), s32[]{:S(2)}) async-start(), calls=%async_computation.3 | async-start | bytes 1310720 | tf_op jit(solution)/shard_map/reduce_scatter | solution.py:17
  8.1 17.3 %collective-permute-start = (bf16[256,1024]{1,0:T(8,128)(2,1)}, bf16[256,1024]{1,0:T(8,128)(2,1)S(1)}, u32[]{:S(2)}, u32[]{:S(2)}) collective-permute-start(bf16[256,1024]{1,0:T(8,128)(2,1)} %param.6), channel_id=1, source_target_pairs={{0,4},{4,8},{8,12},{12,0},{1,5},{5,9},{9,13},{13,1},{2,6},{6,10},{... | collective-permute-start | bytes 1572872 | tf_op jit(solution)/shard_map/ppermute | solution.py:34
  25.3 14.9 %collective-permute-start.1 = (bf16[256,1024]{1,0:T(8,128)(2,1)S(1)}, bf16[256,1024]{1,0:T(8,128)(2,1)S(1)}, u32[]{:S(2)}, u32[]{:S(2)}) collective-permute-start(bf16[256,1024]{1,0:T(8,128)(2,1)S(1)} %collective-permute-done), channel_id=1, source_target_pairs={{0,4},{4,8},{8,12},{12,0},{1,5},{5,9},{9,13},{13,1},{2,6},{6,10},{... | collective-permute-start | bytes 1572872 | tf_op jit(solution)/shard_map/ppermute | solution.py:34
  40.2 26.9 %collective-permute-start.2 = (bf16[256,1024]{1,0:T(8,128)(2,1)S(1)}, bf16[256,1024]{1,0:T(8,128)(2,1)S(1)}, u32[]{:S(2)}, u32[]{:S(2)}) collective-permute-start(bf16[256,1024]{1,0:T(8,128)(2,1)S(1)} %collective-permute-done.1), channel_id=1, source_target_pairs={{0,4},{4,8},{8,12},{12,0},{1,5},{5,9},{9,13},{13,1},{2,6},{6,10},{... | collective-permute-start | bytes 1572872 | tf_op jit(solution)/shard_map/ppermute | solution.py:34
  73.8 42.7 %copy-start = (bf16[128,1024]{1,0:T(8,128)(2,1)S(1)}, bf16[128,1024]{1,0:T(8,128)(2,1)}, u32[]{:S(2)}) copy-start(bf16[128,1024]{1,0:T(8,128)(2,1)} %param.5) | copy-start | bytes 786436
  73.8 45.0 %copy-start.2 = (f32[1024]{0:T(1024)S(1)}, f32[1024]{0:T(1024)}, u32[]{:S(2)}) copy-start(f32[1024]{0:T(1024)} %param.9) | copy-start | bytes 12292
  73.8 45.0 %copy-start.3 = (f32[1024]{0:T(1024)S(1)}, f32[1024]{0:T(1024)}, u32[]{:S(2)}) copy-start(f32[1024]{0:T(1024)} %param.8) | copy-start | bytes 12292
Sparse Core Ops, SparseCore 0:
  8.9 19.4 all-gather.2
  29.9 57.4 all-gather.4
  93.5 22.9 reduce-scatter.1
